TPU v7x, 32 devices: a whole 2x2x4 slice. The times are simulated.
32 devices in a mesh: sp: 8 (over z, x), tp: 4 (over y, core).
Axes of the slice: x: 2, y: 2, z: 4, core: 2. Of those that a mesh axis runs over, the one named last changes fastest.
Arguments:
- tokens: bfloat16 [4096, 2048], P(('sp', 'tp')), may hold values from -6 to 6
- input_norm_scale: bfloat16 [2048], replicated, may hold values from 0.099609375 to 1.8984375
- outer_gate_weight: bfloat16 [2048, 1024], P('sp', 'tp'), may hold values from -0.125 to 0.125
- inner_gate_weight: bfloat16 [2048, 1024], P('sp', 'tp'), may hold values from -0.125 to 0.125
- value_weight_matrix: bfloat16 [2048, 1024], P('sp', 'tp'), may hold values from -0.125 to 0.125
- output_gate_weight: bfloat16 [2048, 1024], P('sp', 'tp'), may hold values from -0.125 to 0.125
- state_input_weight: bfloat16 [2048, 1024], P('sp', 'tp'), may hold values from -0.125 to 0.125
- write_key_weight: bfloat16 [2048, 512], P('sp', 'tp'), may hold values from -0.125 to 0.125
- read_key_weight: bfloat16 [2048, 512], P('sp', 'tp'), may hold values from -0.125 to 0.125
- step_size_weight: bfloat16 [2048, 16], P(None, 'tp'), may hold values from -0.125 to 0.125
- gated_conv_weight: bfloat16 [3, 1024], P(None, 'tp'), may hold values from -3.5 to 3.5
- input_conv_weight: bfloat16 [4, 1024], P(None, 'tp'), may hold values from -3 to 3
- write_conv_weight: bfloat16 [4, 512], P(None, 'tp'), may hold values from -3 to 3
- read_conv_weight: bfloat16 [4, 512], P(None, 'tp'), may hold values from -3 to 3
- step_size_bias: float32 [16], P('tp'), may hold values from -1 to 0.5
- log_decay_rate: float32 [16], P('tp'), may hold values from -16 to -2.5, as said below
- decay_spikes: float32 [16, 4096], P('tp', 'sp'), may hold values from -1 to 0, as said below
- direct_path_weight: float32 [16], P('tp'), may hold values from 0.5 to 2
- head_norm_scale: bfloat16 [1024], P('tp'), may hold values from 0.099609375 to 1.8984375
- conv_output_weight: bfloat16 [1024, 2048], P('tp', 'sp'), may hold values from -0.125 to 0.125
- state_output_weight: bfloat16 [1024, 2048], P('tp', 'sp'), may hold values from -0.125 to 0.125
Outputs:
- mixed: bfloat16 [4096, 2048], P(('sp', 'tp'))
Inputs may be any that keep to these rules, and one draw needn't show every extreme that they name: `log_decay_rate`: one value a head. `decay_spikes`: never positive.
All inputs are finite; a program needn't handle non-finite values.
Results may differ from a plain program's by a relative error of at most 0.017.
Values may be sent and summed in bfloat16 or wider, within the bound.
A program may use at most 128 MiB of HBM per device.

v0:
```python
import jax
import jax.numpy as jnp
from jax import lax
from jax.sharding import PartitionSpec as P

HEAD_DIM = 64
STATE = 128
BLOCK = 64
epsilon = 1e-05
highest = lax.Precision.HIGHEST


def shifted(shard, axis, by):
    devices = lax.axis_size(axis)
    pairs = [(i, i + by) for i in range(devices) if 0 <= i + by < devices]
    return lax.ppermute(shard, axis, pairs)


def prefix(shard, axis, combine, identity):
    devices, index = (lax.axis_size(axis), lax.axis_index(axis))
    everything = jax.tree.map(
        lambda part, kind: lax.all_gather(part.astype(kind), axis),
        shard,
        (jnp.bfloat16, jnp.bfloat16),
    )
    start = jax.tree.map(
        lambda part, zero: jnp.broadcast_to(jnp.asarray(zero, part.dtype), part.shape),
        shard,
        identity,
    )

    def turn(k, before):
        reached = k < index
        new = combine(
            before, jax.tree.map(lambda part, own: part[k].astype(own.dtype), everything, shard)
        )
        return jax.tree.map(lambda a, b: jnp.where(reached, a, b), new, before)

    return lax.fori_loop(0, devices, turn, start)


def causal_taps(values, rim_rows, tap_weights):
    tap_count = tap_weights.shape[0]
    length = values.shape[0]
    padded = jnp.concatenate([rim_rows, values], axis=0)
    running = tap_weights[0] * padded[0:length]
    for offset in range(1, tap_count):
        running = running + tap_weights[offset] * padded[offset : offset + length]
    return running


def combine_states(earlier, later):
    return (earlier[0] * later[0], earlier[1] * later[0][:, None, None] + later[1])


def per_device(
    tokens,
    input_norm_scale,
    outer_gate_weight,
    inner_gate_weight,
    value_weight_matrix,
    output_gate_weight,
    state_input_weight,
    write_key_weight,
    read_key_weight,
    step_size_weight,
    gated_conv_weight,
    input_conv_weight,
    write_conv_weight,
    read_conv_weight,
    step_size_bias,
    log_decay_rate,
    decay_spikes,
    direct_path_weight,
    head_norm_scale,
    conv_output_weight,
    state_output_weight,
):
    token_rows = tokens.astype(jnp.float32)
    scaled = token_rows * lax.rsqrt(
        jnp.mean(token_rows * token_rows, axis=1, keepdims=True) + epsilon
    )
    normed_own = (scaled * input_norm_scale.astype(jnp.float32)).astype(jnp.bfloat16)
    normed = lax.all_gather(normed_own, "tp", axis=0, tiled=True)
    length = normed.shape[0]
    pieces = (
        lax.all_gather(outer_gate_weight, "sp", axis=0, tiled=True),
        lax.all_gather(inner_gate_weight, "sp", axis=0, tiled=True),
        lax.all_gather(value_weight_matrix, "sp", axis=0, tiled=True),
        lax.all_gather(output_gate_weight, "sp", axis=0, tiled=True),
        lax.all_gather(state_input_weight, "sp", axis=0, tiled=True),
        lax.all_gather(write_key_weight, "sp", axis=0, tiled=True),
        lax.all_gather(read_key_weight, "sp", axis=0, tiled=True),
    )
    projected = tuple(
        (jnp.dot(normed, weight_rows, preferred_element_type=jnp.float32) for weight_rows in pieces)
    )
    outer_gate, inner_gate, conv_input, out_gate, state_input, write_keys, read_keys = [
        member.astype(jnp.bfloat16) for member in projected
    ]
    step_raw = jnp.dot(normed, step_size_weight, preferred_element_type=jnp.float32)
    short_rim = gated_conv_weight.shape[0] - 1
    state_rim = input_conv_weight.shape[0] - 1
    rim_rows = shifted(
        (
            inner_gate[length - short_rim :],
            conv_input[length - short_rim :],
            state_input[length - state_rim :],
            write_keys[length - state_rim :],
            read_keys[length - state_rim :],
        ),
        "sp",
        1,
    )
    product = inner_gate.astype(jnp.float32) * conv_input.astype(jnp.float32)
    rim_product = rim_rows[0].astype(jnp.float32) * rim_rows[1].astype(jnp.float32)
    mixer_part = (
        outer_gate.astype(jnp.float32)
        * causal_taps(product, rim_product, gated_conv_weight.astype(jnp.float32))
    ).astype(jnp.bfloat16)
    seq_input = jax.nn.silu(
        causal_taps(
            state_input.astype(jnp.float32),
            rim_rows[2].astype(jnp.float32),
            input_conv_weight.astype(jnp.float32),
        )
    )
    seq_write = jax.nn.silu(
        causal_taps(
            write_keys.astype(jnp.float32),
            rim_rows[3].astype(jnp.float32),
            write_conv_weight.astype(jnp.float32),
        )
    )
    seq_read = jax.nn.silu(
        causal_taps(
            read_keys.astype(jnp.float32),
            rim_rows[4].astype(jnp.float32),
            read_conv_weight.astype(jnp.float32),
        )
    )
    discrete_step = jax.nn.softplus(step_raw + step_size_bias[None, :])
    step_logarithm = discrete_step * (-jnp.exp(log_decay_rate))[None, :] + decay_spikes.T
    heads_here = discrete_step.shape[1]
    groups_here = seq_write.shape[1] // STATE
    per_group = heads_here // groups_here
    blocks = length // BLOCK
    input_blocks = seq_input.reshape(blocks, BLOCK, heads_here, HEAD_DIM)
    weighted = input_blocks * discrete_step.reshape(blocks, BLOCK, heads_here, 1)
    write_blocks = jnp.repeat(
        seq_write.reshape(blocks, BLOCK, groups_here, STATE), per_group, axis=2
    )
    read_blocks = jnp.repeat(seq_read.reshape(blocks, BLOCK, groups_here, STATE), per_group, axis=2)
    cumulative = jnp.cumsum(step_logarithm.reshape(blocks, BLOCK, heads_here), axis=1)
    causal = lax.broadcasted_iota(jnp.int32, (BLOCK, BLOCK), 0) >= lax.broadcasted_iota(
        jnp.int32, (BLOCK, BLOCK), 1
    )
    scores = jnp.einsum("clhm,cshm->clsh", read_blocks, write_blocks, precision=highest)
    damping = jnp.exp(
        jnp.where(
            causal[None, :, :, None],
            cumulative[:, :, None, :] - cumulative[:, None, :, :],
            -jnp.inf,
        )
    )
    within_block = jnp.einsum("clsh,cshp->clhp", scores * damping, weighted, precision=highest)
    to_end = jnp.exp(cumulative[:, -1:, :] - cumulative)
    block_states = jnp.einsum(
        "cshm,cshp->chpm", write_blocks * to_end[..., None], weighted, precision=highest
    )
    block_logs = cumulative[:, -1, :]

    def advance(carried_state, inputs):
        contribution, block_log = inputs
        return (carried_state * jnp.exp(block_log)[:, None, None] + contribution, carried_state)

    own_total, own_before = lax.scan(
        advance, jnp.zeros(block_states.shape[1:], jnp.float32), (block_states, block_logs)
    )
    total_log = jnp.sum(block_logs, axis=0)
    arriving = prefix(
        (jnp.exp(total_log), own_total),
        "sp",
        combine_states,
        (jnp.ones_like(total_log), jnp.zeros_like(own_total)),
    )[1]
    before_logs = jnp.cumsum(block_logs, axis=0) - block_logs
    entering = own_before + jnp.exp(before_logs)[:, :, None, None] * arriving[None]
    from_before = (
        jnp.einsum("clhm,chpm->clhp", read_blocks, entering, precision=highest)
        * jnp.exp(cumulative)[..., None]
    )
    head_out = within_block + from_before + direct_path_weight[None, None, :, None] * input_blocks
    head_out = head_out.reshape(length, heads_here * HEAD_DIM)
    gated_heads = (head_out * jax.nn.silu(out_gate.astype(jnp.float32))).reshape(
        length, heads_here, HEAD_DIM
    )
    normalized = gated_heads * lax.rsqrt(
        jnp.mean(gated_heads * gated_heads, axis=2, keepdims=True) + epsilon
    )
    state_part = (
        normalized.reshape(length, heads_here * HEAD_DIM) * head_norm_scale.astype(jnp.float32)
    ).astype(jnp.bfloat16)
    wide_mixer, wide_state = (
        lax.all_gather(conv_output_weight, "sp", axis=1, tiled=True),
        lax.all_gather(state_output_weight, "sp", axis=1, tiled=True),
    )
    return lax.psum_scatter(
        (
            jnp.dot(mixer_part, wide_mixer, preferred_element_type=jnp.float32)
            + jnp.dot(state_part, wide_state, preferred_element_type=jnp.float32)
        ).astype(jnp.bfloat16),
        "tp",
        scatter_dimension=0,
        tiled=True,
    )


def solution(mesh):
    placed = (
        P(("sp", "tp"), None),
        P(),
        P("sp", "tp"),
        P("sp", "tp"),
        P("sp", "tp"),
        P("sp", "tp"),
        P("sp", "tp"),
        P("sp", "tp"),
        P("sp", "tp"),
        P(None, "tp"),
        P(None, "tp"),
        P(None, "tp"),
        P(None, "tp"),
        P(None, "tp"),
        P("tp"),
        P("tp"),
        P("tp", "sp"),
        P("tp"),
        P("tp"),
        P("tp", "sp"),
        P("tp", "sp"),
    )
    return jax.shard_map(
        per_device, mesh=mesh, in_specs=placed, out_specs=P(("sp", "tp"), None), check_vma=False
    )
```

profile of v0, /device:TPU:0, one launch (start us, length us, event | category | flops | bytes accessed | tf_op | source)
XLA Modules:
  0.0 369.9 jit_solution(7055636501463184764)
XLA Ops:
  6.6 0.7 convert_element_type.131
  7.4 1.3 fusion.12
  8.7 2.0 fusion.14
  10.8 0.7 all-gather.21.cloned.1.call-update
  14.0 0.7 all-gather.23.cloned.1.call-update
  14.8 0.7 all-gather.25.cloned.1.call-update
  15.6 35.2 %all_gather.46 = bf16[2048,128]{1,0:T(8,128)(2,1)} all-gather(bf16[256,128]{1,0:T(8,128)(2,1)S(1)} %copy-done.7), channel_id=1, replica_groups=mesh['sp'=8,'tp'=4] {'sp'}, dimensions={0}, use_global_device_ids=true | all-gather | bytes 589824 | tf_op jit(solution)/shard_map/all_gather | solution.py:92
  51.4 33.7 %all_gather.47 = bf16[2048,128]{1,0:T(8,128)(2,1)} all-gather(bf16[256,128]{1,0:T(8,128)(2,1)S(1)} %copy-done.8), channel_id=1, replica_groups=mesh['sp'=8,'tp'=4] {'sp'}, dimensions={0}, use_global_device_ids=true | all-gather | bytes 589824 | tf_op jit(solution)/shard_map/all_gather | solution.py:93
  87.5 2.4 bitcast_add_fusion.1
  90.2 6.3 %fusion.75 = f32[8,64,4]{2,0,1:T(8,128)S(1)} fusion(f32[8,64,4]{2,0,1:T(8,128)S(1)} %copy.54), kind=kOutput, calls=%fused_computation.130 | output fusion | flops 129024 | bytes 16384 | tf_op jit(solution)/shard_map/jit(cumsum)/reduce_window_sum | solution.py:154
  96.7 1.9 fusion.73
  98.7 4.0 %collective-permute-start.2 = (bf16[3,256]{1,0:T(4,128)(2,1)S(1)}, bf16[3,256]{1,0:T(4,128)(2,1)S(1)}, u32[]{:S(2)}, u32[]{:S(2)}) collective-permute-start(bf16[3,256]{1,0:T(4,128)(2,1)S(1)} %slice.137), channel_id=1, source_target_pairs={{0,4},{4,8},{8,12},{12,16},{16,20},{20,24},{24,28},{1,5},{5,9},{9,... | collective-permute-start | bytes 4616 | tf_op jit(solution)/shard_map/ppermute | solution.py:16
  102.7 1.7 fusion.72
  105.0 2.5 collective-permute-start.3
  107.7 0.9 fusion.68
  108.7 13.8 %all-gather.15.cloned.1.call-done = bf16[2048,256]{1,0:T(8,128)(2,1)} async-done(((bf16[256,256]{1,0:T(8,128)(2,1)}), bf16[2048,256]{1,0:T(8,128)(2,1)}) %all-gather.15.cloned.1.call-update) | async-done | bytes 1048592 | tf_op jit(solution)/shard_map/all_gather | solution.py:88
  122.6 1.9 convolution_convert_fusion.3
  125.3 2.5 fusion.71
  127.9 35.7 %all-gather.17.cloned.1.call-done = bf16[2048,256]{1,0:T(8,128)(2,1)} async-done(((bf16[256,256]{1,0:T(8,128)(2,1)}), bf16[2048,256]{1,0:T(8,128)(2,1)}) %all-gather.17.cloned.1.call-update) | async-done | bytes 1048592 | tf_op jit(solution)/shard_map/all_gather | solution.py:89
  163.6 2.9 convert_multiply_fusion.2
  166.4 1.1 copy.60
  167.5 19.2 %all-reduce = bf16[32]{0:T(256)(128)(2,1)S(1)} all-reduce(bf16[32]{0:T(256)(128)(2,1)S(1)} %dynamic-update-slice), channel_id=2, replica_groups=mesh['sp'=8,'tp'=4] {'sp'}, use_global_device_ids=true, to_apply=%add | all-reduce | flops 32 | bytes 128
  186.9 1.2 slice.150
  188.1 2.5 collective-permute-start.4
  190.8 0.7 slice.131
  191.5 1.5 collective-permute-start.1
  193.0 2.2 collective-permute-start
  195.9 0.8 divide_multiply_fusion.2
  197.3 1.5 divide_multiply_fusion.1
  198.9 2.7 fusion.5
  201.6 3.0 all-gather.13.cloned.1.call-done
  204.6 40.0 %all-gather.19.cloned.1.call-done = bf16[256,2048]{1,0:T(8,128)(2,1)} async-done(((bf16[256,256]{1,0:T(8,128)(2,1)}), bf16[256,2048]{1,0:T(8,128)(2,1)}) %all-gather.19.cloned.1.call-update) | async-done | bytes 1048592 | tf_op jit(solution)/shard_map/all_gather | solution.py:205
  244.6 6.3 %fusion.11 = f32[512,2048]{1,0:T(8,128)} fusion(bf16[256,2048]{1,0:T(8,128)(2,1)} %all-gather.19.cloned.1.call-done, bf16[512,2048]{1,0:T(8,128)(2,1)S(1)} %copy-done.1, bf16[2048,256]{1,0:T(8,128)(2,1)} %all-gather.13.cloned.1.call-done, f32[2,256]{1,0:T(2,128)S(1)} %convert_multiply_fusion.3, f32[512,256]{1,0:T(8,128)} %get-tuple-element.220, ...), kind=kOutput, calls=%fused_computation.27 | convolution fusion | flops 1075183616 | bytes 8918016 | tf_op jit(solution)/shard_map/dot_general | solution.py:210
  250.9 1.1 divide_multiply_fusion
  252.0 2.5 reshape.111
  254.6 1.5 copy.53
  256.1 3.2 fusion.17
  259.4 13.5 %while.27 = (s32[]{:T(128)}, f32[4,64,128]{2,1,0:T(8,128)S(1)}, f32[8,4,64,128]{3,2,1,0:T(8,128)}, f32[8,4]{1,0:T(8,128)S(1)}, f32[8,4,64,128]{3,2,1,0:T(8,128)}, /*index=5*/s32[]{:T(128)}, s32[]{:T(128)}) while((s32[]{:T(128)}, f32[4,64,128]{2,1,0:T(8,128)S(1)}, f32[8,4,64,128]{3,2,1,0:T(8,128)}, f32[8,4]{1,0:T(8,128)S(1)}, ...), condition=%wide.region_3.4_spmd.clone, body=%wide.region_2.3_spmd.clone.sunk | while | flops 131075 | bytes 656016 | solution.py:177
  260.0 1.0 bitcast_add_fusion.3
  261.7 1.0 bitcast_add_fusion.3
  263.4 1.0 bitcast_add_fusion.3
  265.1 1.0 bitcast_add_fusion.3
  266.8 1.0 bitcast_add_fusion.3
  268.4 1.0 bitcast_add_fusion.3
  270.1 1.0 bitcast_add_fusion.3
  271.8 1.0 bitcast_add_fusion.3
  272.9 33.8 %all-gather.1 = bf16[32,64,128]{2,1,0:T(8,128)(2,1)} all-gather(bf16[4,64,128]{2,1,0:T(8,128)(2,1)S(1)} %convert_element_type.157), channel_id=3, replica_groups=mesh['sp'=8,'tp'=4] {'sp'}, dimensions={0}, use_global_device_ids=true | all-gather | bytes 589824 | tf_op jit(solution)/shard_map/all_gather | solution.py:22
  306.6 7.7 %while.28 = (s32[]{:T(128)}, f32[4,64,128]{2,1,0:T(8,128)S(1)}, s32[]{:T(128)}, bf16[8,4]{1,0:T(8,128)(2,1)S(1)}, bf16[8,4,64,128]{3,2,1,0:T(8,128)(2,1)}, /*index=5*/s32[]{:T(128)}, s32[]{:T(128)}) while((s32[]{:T(128)}, f32[4,64,128]{2,1,0:T(8,128)S(1)}, s32[]{:T(128)}, bf16[8,4]{1,0:T(8,128)(2,1)S(1)}, ...), condition=%wide.region_7.8_spmd.clone, body=%wide.region_6.7_spmd.clone.sunk | while | flops 163848 | bytes 327825 | solution.py:39
  306.6 0.9 fusion.99
  307.6 0.9 fusion.99
  308.6 0.9 fusion.99
  309.5 0.9 fusion.99
  310.5 0.9 fusion.99
  311.5 0.9 fusion.99
  312.5 0.9 fusion.99
  313.4 0.9 fusion.99
  314.4 2.5 convolution_bitcast_fusion.1
  316.9 2.9 fusion.6
  319.8 1.6 copy.65
  321.4 1.4 reshape.117
  322.9 2.1 fusion.74
  325.5 2.9 all-gather.25.cloned.1.call-done
  328.4 4.6 %add_convert_fusion = bf16[512,2048]{1,0:T(8,128)(2,1)} fusion(f32[512,2048]{1,0:T(8,128)} %fusion.11, bf16[256,2048]{1,0:T(8,128)(2,1)} %all-gather.25.cloned.1.call-done, f32[512,256]{1,0:T(8,128)S(1)} %get-tuple-element.231, f32[512,256]{1,0:T(8,128)S(1)} %copy.68, f32[256]{0:T(256)S(1)} %copy-done.12), kind=kOutput, calls=%fused_computation.8 | convolution fusion | flops 539361280 | bytes 8389632 | tf_op jit(solution)/shard_map/dot_general | solution.py:211
  333.1 30.3 %reduce-scatter.2.cloned.1.call-done = bf16[128,2048]{1,0:T(8,128)(2,1)} async-done(((bf16[512,2048]{1,0:T(8,128)(2,1)}), bf16[128,2048]{1,0:T(8,128)(2,1)}) %reduce-scatter.2.cloned.1.call-update) | async-done | bytes 524304 | tf_op jit(solution)/shard_map/reduce_scatter | solution.py:208
  (132 shorter events, 14.9 us)
Async XLA Ops:
  6.5 80.9 %copy-start = (bf16[2048,4]{0,1:T(4,128)(2,1)S(1)}, bf16[2048,4]{0,1:T(4,128)(2,1)}, u32[]{:S(2)}) copy-start(bf16[2048,4]{0,1:T(4,128)(2,1)} %param.34) | copy-start | bytes 49156
  6.5 9.0 %copy-start.10 = (bf16[4,256]{1,0:T(4,128)(2,1)S(1)}, bf16[4,256]{1,0:T(4,128)(2,1)}, u32[]{:S(2)}) copy-start(bf16[4,256]{1,0:T(4,128)(2,1)} %param.36) | copy-start | bytes 6148
  6.5 9.0 %copy-start.7 = (bf16[256,128]{1,0:T(8,128)(2,1)S(1)}, bf16[256,128]{1,0:T(8,128)(2,1)}, u32[]{:S(2)}) copy-start(bf16[256,128]{1,0:T(8,128)(2,1)} %param.32) | copy-start | bytes 196612
  6.5 44.3 %copy-start.13 = (bf16[4,128]{1,0:T(4,128)(2,1)S(1)}, bf16[4,128]{1,0:T(4,128)(2,1)}, u32[]{:S(2)}) copy-start(bf16[4,128]{1,0:T(4,128)(2,1)} %param.37) | copy-start | bytes 3076
  6.5 44.8 %copy-start.18 = (f32[4]{0:T(128)S(1)}, f32[4]{0:T(128)}, u32[]{:S(2)}) copy-start(f32[4]{0:T(128)} %param.40) | copy-start | bytes 52
  6.5 44.8 %copy-start.8 = (bf16[256,128]{1,0:T(8,128)(2,1)S(1)}, bf16[256,128]{1,0:T(8,128)(2,1)}, u32[]{:S(2)}) copy-start(bf16[256,128]{1,0:T(8,128)(2,1)} %param.33) | copy-start | bytes 196612
  6.6 80.9 %all-gather.11.cloned.1.call-start = ((), (), s32[]{:S(2)}) async-start(), calls=%async_computation.1 | async-start | bytes 2621440 | tf_op jit(solution)/shard_map/all_gather | solution.py:84
  7.3 77.7 %copy-start.14 = (bf16[4,128]{1,0:T(4,128)(2,1)S(1)}, bf16[4,128]{1,0:T(4,128)(2,1)}, u32[]{:S(2)}) copy-start(bf16[4,128]{1,0:T(4,128)(2,1)} %param.38) | copy-start | bytes 3076
  7.3 78.3 %copy-start.11 = (bf16[3,256]{1,0:T(4,128)(2,1)S(1)}, bf16[3,256]{1,0:T(4,128)(2,1)}, u32[]{:S(2)}) copy-start(bf16[3,256]{1,0:T(4,128)(2,1)} %param.35) | copy-start | bytes 4612
  7.4 78.3 %copy-start.19 = (bf16[256]{0:T(256)(128)(2,1)S(1)}, bf16[256]{0:T(256)(128)(2,1)}, u32[]{:S(2)}) copy-start(bf16[256]{0:T(256)(128)(2,1)} %param.43) | copy-start | bytes 1540
  7.4 78.9 %copy-start.20 = (u32[32]{0:T(128)S(1)}, u32[32]{0:T(128)}, u32[]{:S(2)}) copy-start(u32[32]{0:T(128)} %constant.73) | copy-start | bytes 388
  7.4 80.1 %copy-start.9 = (f32[4,512]{1,0:T(4,128)S(1)}, f32[4,512]{1,0:T(4,128)}, u32[]{:S(2)}) copy-start(f32[4,512]{1,0:T(4,128)} %param.41) | copy-start | bytes 24580
  7.4 80.1 %copy-start.16 = (f32[4]{0:T(128)S(1)}, f32[4]{0:T(128)}, u32[]{:S(2)}) copy-start(f32[4]{0:T(128)} %param.39) | copy-start | bytes 52
  10.7 86.0 %all-gather.21.cloned.1.call-start = ((), (), s32[]{:S(2)}) async-start(), calls=%async_computation.6 | async-start | bytes 1179648 | tf_op jit(solution)/shard_map/all_gather | solution.py:91
  11.5 111.1 %all-gather.15.cloned.1.call-start = ((), (), s32[]{:S(2)}) async-start(), calls=%async_computation.3 | async-start | bytes 1179648 | tf_op jit(solution)/shard_map/all_gather | solution.py:88
  12.2 151.3 %all-gather.17.cloned.1.call-start = ((), (), s32[]{:S(2)}) async-start(), calls=%async_computation.4 | async-start | bytes 1179648 | tf_op jit(solution)/shard_map/all_gather | solution.py:89
  12.8 191.8 %all-gather.13.cloned.1.call-start = ((), (), s32[]{:S(2)}) async-start(), calls=%async_computation.2 | async-start | bytes 1179648 | tf_op jit(solution)/shard_map/all_gather | solution.py:87
  13.4 231.3 %all-gather.19.cloned.1.call-start = ((), (), s32[]{:S(2)}) async-start(), calls=%async_computation.5 | async-start | bytes 1179648 | tf_op jit(solution)/shard_map/all_gather | solution.py:205
  14.0 308.9 %all-gather.23.cloned.1.call-start = ((), (), s32[]{:S(2)}) async-start(), calls=%async_computation.7 | async-start | bytes 1179648 | tf_op jit(solution)/shard_map/all_gather | solution.py:90
  14.7 313.7 %all-gather.25.cloned.1.call-start = ((), (), s32[]{:S(2)}) async-start(), calls=%async_computation.8 | async-start | bytes 1179648 | tf_op jit(solution)/shard_map/all_gather | solution.py:206
  15.5 347.9 %reduce-scatter.2.cloned.1.call-start = ((), (), s32[]{:S(2)}) async-start(), calls=%async_computation.9 | async-start | bytes 2621440 | tf_op jit(solution)/shard_map/reduce_scatter | solution.py:208
  87.5 9.2 %copy-start.1 = (bf16[512,2048]{1,0:T(8,128)(2,1)S(1)}, bf16[512,2048]{1,0:T(8,128)(2,1)}, u32[]{:S(2)}) copy-start(bf16[512,2048]{1,0:T(8,128)(2,1)} %all-gather.11.cloned.1.call-done) | copy-start | bytes 6291460
  98.7 152.2 %collective-permute-start.2 = (bf16[3,256]{1,0:T(4,128)(2,1)S(1)}, bf16[3,256]{1,0:T(4,128)(2,1)S(1)}, u32[]{:S(2)}, u32[]{:S(2)}) collective-permute-start(bf16[3,256]{1,0:T(4,128)(2,1)S(1)} %slice.137), channel_id=1, source_target_pairs={{0,4},{4,8},{8,12},{12,16},{16,20},{20,24},{24,28},{1,5},{5,9},{9,... | collective-permute-start | bytes 4616 | tf_op jit(solution)/shard_map/ppermute | solution.py:16
  105.0 90.2 %collective-permute-start.3 = (bf16[3,128]{1,0:T(4,128)(2,1)}, bf16[3,128]{1,0:T(4,128)(2,1)}, u32[]{:S(2)}, u32[]{:S(2)}) collective-permute-start(bf16[3,128]{1,0:T(4,128)(2,1)} %slice.145), channel_id=1, source_target_pairs={{0,4},{4,8},{8,12},{12,16},{16,20},{20,24},{24,28},{1,5},{5,9},{9,... | collective-permute-start | bytes 2312 | tf_op jit(solution)/shard_map/ppermute | solution.py:16
  124.5 0.8 copy-start.17
  127.9 62.7 %copy-start.5 = (f32[8,64,4]{2,0,1:T(8,128)S(1)}, f32[8,64,4]{2,0,1:T(8,128)}, u32[]{:S(2)}) copy-start(f32[8,64,4]{2,0,1:T(8,128)} %get-tuple-element.203) | copy-start | bytes 24580
  188.1 8.6 %collective-permute-start.4 = (bf16[3,128]{1,0:T(4,128)(2,1)}, bf16[3,128]{1,0:T(4,128)(2,1)}, u32[]{:S(2)}, u32[]{:S(2)}) collective-permute-start(bf16[3,128]{1,0:T(4,128)(2,1)} %slice.150), channel_id=1, source_target_pairs={{0,4},{4,8},{8,12},{12,16},{16,20},{20,24},{24,28},{1,5},{5,9},{9,... | collective-permute-start | bytes 2312 | tf_op jit(solution)/shard_map/ppermute | solution.py:16
  191.5 10.1 %collective-permute-start.1 = (bf16[2,256]{1,0:T(2,128)(2,1)S(1)}, bf16[2,256]{1,0:T(2,128)(2,1)S(1)}, u32[]{:S(2)}, u32[]{:S(2)}) collective-permute-start(bf16[2,256]{1,0:T(2,128)(2,1)S(1)} %slice.131), channel_id=1, source_target_pairs={{0,4},{4,8},{8,12},{12,16},{16,20},{20,24},{24,28},{1,5},{5,9},{9,... | collective-permute-start | bytes 3080 | tf_op jit(solution)/shard_map/ppermute | solution.py:16
  193.0 8.6 %collective-permute-start = (bf16[2,256]{1,0:T(2,128)(2,1)}, bf16[2,256]{1,0:T(2,128)(2,1)S(1)}, u32[]{:S(2)}, u32[]{:S(2)}) collective-permute-start(bf16[2,256]{1,0:T(2,128)(2,1)} %slice.130), channel_id=1, source_target_pairs={{0,4},{4,8},{8,12},{12,16},{16,20},{20,24},{24,28},{1,5},{5,9},{9,... | collective-permute-start | bytes 3080 | tf_op jit(solution)/shard_map/ppermute | solution.py:16
  196.7 2.2 copy-start.4
  198.9 52.0 %copy-start.2 = (f32[512,128]{1,0:T(8,128)}, f32[512,128]{1,0:T(8,128)S(1)}, u32[]{:S(2)}) copy-start(f32[512,128]{1,0:T(8,128)S(1)} %divide_multiply_fusion.1) | copy-start | bytes 786436
  306.6 10.3 %copy-start.15 = (f32[4]{0:T(128)S(1)}, f32[4]{0:T(128)}, u32[]{:S(2)}) copy-start(f32[4]{0:T(128)} %param.42) | copy-start | bytes 52
  314.4 2.5 copy-start.3
  314.4 2.5 copy-start.6
  325.0 3.5 copy-start.12
Sparse Core Ops, SparseCore 0:
  10.9 25.2 all-gather.10
  38.3 43.1 all-gather.20
  83.6 38.8 all-gather.14
  124.5 38.9 all-gather.16
  165.5 39.0 all-gather.12
  206.5 38.0 all-gather.18
  246.8 41.4 all-gather.22
  290.3 38.0 all-gather.24
  333.2 30.1 reduce-scatter.1
where the time goes:
time: 371 us; the launch traced here: 370 us
  waiting for transfers between devices  130 us (35%)
  blocking collectives  122 us (33%)
  matrix products  37.7 us (10%)
  other arithmetic  37.6 us (10%)
  local copies, waits for them, and re-layouts  14.8 us (4%)
  between operations  14.3 us (4%)
  starting transfers between devices  13 us (4%)
    all_gather x1, waiting for transfers between devices, per_device(): lax.all_gather(conv_output_weight, 'sp', axis=1, tiled=True)  40 us
    all_gather x1, waiting for transfers between devices, per_device(): lax.all_gather(value_weight_matrix, 'sp', axis=0, tiled=True)  35.7 us
    all_gather x1, blocking collectives, per_device(): lax.all_gather(write_key_weight, 'sp', axis=0, tiled=True)  35.2 us
    all_gather x1, blocking collectives, prefix(): lax.all_gather(part.astype(kind), axis)  33.8 us
    all_gather x1, blocking collectives, per_device(): lax.all_gather(read_key_weight, 'sp', axis=0, tiled=True)  33.7 us
    reduce_scatter x1, waiting for transfers between devices, per_device(): lax.psum_scatter((jnp.dot(mixer_part, wide_mixer, preferred_element_type=...  30.3 us
    unnamed x1, blocking collectives  19.2 us
    all_gather x1, waiting for transfers between devices, per_device(): lax.all_gather(inner_gate_weight, 'sp', axis=0, tiled=True)  13.8 us
  transfers between devices with their start and end apart: 14, of which 6 were waited for; matrix products, arithmetic and copies ran while one was open for 22% of the time, Pallas kernels for 0%

commit v1 on v0

--- a/solution.py
+++ b/solution.py
@@ -202,7 +202,7 @@
         normalized.reshape(length, heads_here * HEAD_DIM) * head_norm_scale.astype(jnp.float32)
     ).astype(jnp.bfloat16)
     wide_mixer, wide_state = (
-        lax.all_gather(conv_output_weight, "sp", axis=1, tiled=True),
+        jnp.concatenate(lax.all_gather(conv_output_weight, "sp"), axis=1),
         lax.all_gather(state_output_weight, "sp", axis=1, tiled=True),
     )
     return lax.psum_scatter(

time: 371 us -> 371 us (level)
  local copies, waits for them, and re-layouts: 14.8 us -> 20.6 us
  waiting for transfers between devices: 130 us -> 125 us
    all_gather x1, waiting for transfers between devices: 40 us -> 0.02 us  [per_device(): lax.all_gather(conv_output_weight, 'sp')]
    all_gather x1, waiting for transfers between devices: 0.01 us -> 24.8 us  [per_device(): lax.all_gather(state_input_weight, 'sp', axis=0, tiled=True)]
    all_gather x1, waiting for transfers between devices: 13.8 us -> 27.8 us  [per_device(): lax.all_gather(inner_gate_weight, 'sp', axis=0, tiled=True)]
    another operation x1, other arithmetic: 6.33 us -> 1.02 us  [per_device(): jnp.cumsum(step_logarithm.reshape(blocks, BLOCK, heads_here), axis=1)]
  transfers between devices with their start and end apart: 14 -> 14, of which waited for: 6 -> 5; matrix products, arithmetic and copies ran while one was open for 22% -> 24% of each run, Pallas kernels for 0% -> 0%
where the time goes in v1:
time: 371 us; the launch traced here: 369 us
  waiting for transfers between devices  125 us (34%)
  blocking collectives  123 us (33%)
  matrix products  37.9 us (10%)
  other arithmetic  35.1 us (9%)
  local copies, waits for them, and re-layouts  20.6 us (6%)
  between operations  14.3 us (4%)
  starting transfers between devices  12.7 us (3%)
    all_gather x1, blocking collectives, per_device(): lax.all_gather(write_key_weight, 'sp', axis=0, tiled=True)  35.9 us
    all_gather x1, waiting for transfers between devices, per_device(): lax.all_gather(value_weight_matrix, 'sp', axis=0, tiled=True)  35.1 us
    all_gather x1, blocking collectives, prefix(): lax.all_gather(part.astype(kind), axis)  33.9 us
    all_gather x1, blocking collectives, per_device(): lax.all_gather(read_key_weight, 'sp', axis=0, tiled=True)  33.4 us
    reduce_scatter x1, waiting for transfers between devices, per_device(): lax.psum_scatter((jnp.dot(mixer_part, wide_mixer, preferred_element_type=...  30.3 us
    all_gather x1, waiting for transfers between devices, per_device(): lax.all_gather(inner_gate_weight, 'sp', axis=0, tiled=True)  27.8 us
    all_gather x1, waiting for transfers between devices, per_device(): lax.all_gather(state_input_weight, 'sp', axis=0, tiled=True)  24.8 us
    unnamed x1, blocking collectives  19.7 us
  transfers between devices with their start and end apart: 14, of which 5 were waited for; matrix products, arithmetic and copies ran while one was open for 24% of the time, Pallas kernels for 0%

profile of v1, /device:TPU:0, one launch (start us, length us, event | category | flops | bytes accessed | tf_op | source)
XLA Modules:
  0.0 368.9 jit_solution(5824901739142581647)
XLA Ops:
  8.1 1.2 fusion.12
  9.3 2.0 fusion.14
  15.5 35.9 %all_gather.50 = bf16[2048,128]{1,0:T(8,128)(2,1)} all-gather(bf16[256,128]{1,0:T(8,128)(2,1)S(1)} %copy-done.8), channel_id=1, replica_groups=mesh['sp'=8,'tp'=4] {'sp'}, dimensions={0}, use_global_device_ids=true | all-gather | bytes 589824 | tf_op jit(solution)/shard_map/all_gather | solution.py:92
  52.0 33.4 %all_gather.51 = bf16[2048,128]{1,0:T(8,128)(2,1)} all-gather(bf16[256,128]{1,0:T(8,128)(2,1)S(1)} %copy-done.9), channel_id=1, replica_groups=mesh['sp'=8,'tp'=4] {'sp'}, dimensions={0}, use_global_device_ids=true | all-gather | bytes 589824 | tf_op jit(solution)/shard_map/all_gather | solution.py:93
  87.8 1.5 copy.70
  89.4 2.4 bitcast_add_fusion.1
  91.9 0.9 copy.73
  92.8 1.0 fusion.75
  94.5 1.1 copy.74
  95.6 24.8 %all-gather.20.cloned.1.call-done = bf16[2048,256]{1,0:T(8,128)(2,1)} async-done(((bf16[256,256]{1,0:T(8,128)(2,1)}), bf16[2048,256]{1,0:T(8,128)(2,1)}) %all-gather.20.cloned.1.call-update) | async-done | bytes 1048592 | tf_op jit(solution)/shard_map/all_gather | solution.py:91
  120.4 2.8 fusion.73
  123.2 2.5 collective-permute-start.2
  125.7 1.4 fusion.72
  127.7 3.7 collective-permute-start.3
  131.5 1.8 fusion.68
  133.6 27.8 %all-gather.16.cloned.1.call-done = bf16[2048,256]{1,0:T(8,128)(2,1)} async-done(((bf16[256,256]{1,0:T(8,128)(2,1)}), bf16[2048,256]{1,0:T(8,128)(2,1)}) %all-gather.16.cloned.1.call-update) | async-done | bytes 1048592 | tf_op jit(solution)/shard_map/all_gather | solution.py:88
  161.4 1.9 convolution_convert_fusion.3
  164.8 2.5 fusion.71
  167.3 35.1 %all-gather.18.cloned.1.call-done = bf16[2048,256]{1,0:T(8,128)(2,1)} async-done(((bf16[256,256]{1,0:T(8,128)(2,1)}), bf16[2048,256]{1,0:T(8,128)(2,1)}) %all-gather.18.cloned.1.call-update) | async-done | bytes 1048592 | tf_op jit(solution)/shard_map/all_gather | solution.py:89
  202.4 2.9 convert_multiply_fusion.2
  205.2 1.1 copy.79
  206.3 19.7 %all-reduce = bf16[32]{0:T(256)(128)(2,1)} all-reduce(bf16[32]{0:T(256)(128)(2,1)S(1)} %dynamic-update-slice), channel_id=3, replica_groups=mesh['sp'=8,'tp'=4] {'sp'}, use_global_device_ids=true, to_apply=%add | all-reduce | flops 32 | bytes 128
  226.1 0.7 reshape.129
  226.9 1.3 slice.150
  228.1 2.5 collective-permute-start.4
  230.7 1.1 copy.82
  232.5 1.5 collective-permute-start.1
  234.0 2.2 collective-permute-start
  236.8 1.7 divide_multiply_fusion.2
  239.3 1.6 divide_multiply_fusion.1
  240.9 0.7 copy-done.4
  241.6 2.7 fusion.5
  244.4 6.0 %fusion.11 = f32[512,2048]{1,0:T(8,128)} fusion(bf16[256,2048]{0,1:T(8,128)(2,1)S(1)} %bitcast.98, bf16[512,2048]{1,0:T(8,128)(2,1)S(1)} %copy-done.1, bf16[2048,256]{1,0:T(8,128)(2,1)} %all-gather.14.cloned.1.call-done, f32[2,256]{1,0:T(2,128)S(1)} %convert_multiply_fusion.3, f32[512,256]{1,0:T(8,128)} %get-tuple-element.225, f32[256]{0:T(256)S(1)} %bitcast.110, ...), kind=kOutput, calls=%fused_computation.27 | convolution fusion | flops 1075183616 | bytes 8918016 | tf_op jit(solution)/shard_map/dot_general | solution.py:210
  250.4 2.0 divide_multiply_fusion
  252.4 1.5 reshape.119
  253.9 1.5 copy.72
  255.5 3.2 fusion.17
  258.7 13.4 %while.27 = (s32[]{:T(128)}, f32[4,64,128]{2,1,0:T(8,128)S(1)}, f32[8,4,64,128]{3,2,1,0:T(8,128)}, f32[8,4]{1,0:T(8,128)S(1)}, f32[8,4,64,128]{3,2,1,0:T(8,128)}, /*index=5*/s32[]{:T(128)}, s32[]{:T(128)}) while((s32[]{:T(128)}, f32[4,64,128]{2,1,0:T(8,128)S(1)}, f32[8,4,64,128]{3,2,1,0:T(8,128)}, f32[8,4]{1,0:T(8,128)S(1)}, ...), condition=%wide.region_3.4_spmd.clone, body=%wide.region_2.3_spmd.clone.sunk | while | flops 131075 | bytes 656016 | solution.py:177
  259.4 1.0 bitcast_add_fusion.3
  261.1 1.0 bitcast_add_fusion.3
  262.7 1.0 bitcast_add_fusion.3
  264.4 1.0 bitcast_add_fusion.3
  266.1 1.0 bitcast_add_fusion.3
  267.8 1.0 bitcast_add_fusion.3
  269.4 1.0 bitcast_add_fusion.3
  271.1 1.0 bitcast_add_fusion.3
  272.2 33.9 %all-gather.2 = bf16[32,64,128]{2,1,0:T(8,128)(2,1)} all-gather(bf16[4,64,128]{2,1,0:T(8,128)(2,1)S(1)} %convert_element_type.157), channel_id=4, replica_groups=mesh['sp'=8,'tp'=4] {'sp'}, dimensions={0}, use_global_device_ids=true | all-gather | bytes 589824 | tf_op jit(solution)/shard_map/all_gather | solution.py:22
  306.1 7.7 %while.28 = (s32[]{:T(128)}, f32[4,64,128]{2,1,0:T(8,128)S(1)}, s32[]{:T(128)}, bf16[8,4]{1,0:T(8,128)(2,1)S(1)}, bf16[8,4,64,128]{3,2,1,0:T(8,128)(2,1)}, /*index=5*/s32[]{:T(128)}, s32[]{:T(128)}) while((s32[]{:T(128)}, f32[4,64,128]{2,1,0:T(8,128)S(1)}, s32[]{:T(128)}, bf16[8,4]{1,0:T(8,128)(2,1)S(1)}, ...), condition=%wide.region_7.8_spmd.clone, body=%wide.region_6.7_spmd.clone.sunk | while | flops 163848 | bytes 327825 | solution.py:39
  306.1 0.9 fusion.99
  307.1 0.9 fusion.99
  308.0 0.9 fusion.99
  309.0 0.9 fusion.99
  310.0 0.9 fusion.99
  310.9 0.9 fusion.99
  311.9 0.9 fusion.99
  312.9 0.9 fusion.99
  313.8 2.5 convolution_bitcast_fusion.1
  316.4 2.9 fusion.6
  319.3 1.6 copy.84
  320.9 1.4 reshape.125
  322.3 2.1 fusion.74
  325.0 2.5 all-gather.24.cloned.1.call-done
  327.4 4.6 %add_convert_fusion = bf16[512,2048]{1,0:T(8,128)(2,1)} fusion(f32[512,2048]{1,0:T(8,128)} %fusion.11, bf16[256,2048]{1,0:T(8,128)(2,1)} %all-gather.24.cloned.1.call-done, f32[512,256]{1,0:T(8,128)S(1)} %get-tuple-element.236, f32[512,256]{1,0:T(8,128)S(1)} %copy.87, f32[256]{0:T(256)S(1)} %copy-done.13), kind=kOutput, calls=%fused_computation.8 | convolution fusion | flops 539361280 | bytes 8389632 | tf_op jit(solution)/shard_map/dot_general | solution.py:211
  332.1 30.3 %reduce-scatter.2.cloned.1.call-done = bf16[128,2048]{1,0:T(8,128)(2,1)} async-done(((bf16[512,2048]{1,0:T(8,128)(2,1)}), bf16[128,2048]{1,0:T(8,128)(2,1)}) %reduce-scatter.2.cloned.1.call-update) | async-done | bytes 524304 | tf_op jit(solution)/shard_map/reduce_scatter | solution.py:208
  (135 shorter events, 19.3 us)
Async XLA Ops:
  6.5 82.8 %copy-start = (bf16[2048,4]{0,1:T(4,128)(2,1)S(1)}, bf16[2048,4]{0,1:T(4,128)(2,1)}, u32[]{:S(2)}) copy-start(bf16[2048,4]{0,1:T(4,128)(2,1)} %param.34) | copy-start | bytes 49156
  6.5 8.9 %copy-start.11 = (bf16[4,256]{1,0:T(4,128)(2,1)S(1)}, bf16[4,256]{1,0:T(4,128)(2,1)}, u32[]{:S(2)}) copy-start(bf16[4,256]{1,0:T(4,128)(2,1)} %param.36) | copy-start | bytes 6148
  6.5 8.9 %copy-start.8 = (bf16[256,128]{1,0:T(8,128)(2,1)S(1)}, bf16[256,128]{1,0:T(8,128)(2,1)}, u32[]{:S(2)}) copy-start(bf16[256,128]{1,0:T(8,128)(2,1)} %param.32) | copy-start | bytes 196612
  6.5 44.9 %copy-start.14 = (bf16[4,128]{1,0:T(4,128)(2,1)S(1)}, bf16[4,128]{1,0:T(4,128)(2,1)}, u32[]{:S(2)}) copy-start(bf16[4,128]{1,0:T(4,128)(2,1)} %param.37) | copy-start | bytes 3076
  6.5 45.4 %copy-start.19 = (f32[4]{0:T(128)S(1)}, f32[4]{0:T(128)}, u32[]{:S(2)}) copy-start(f32[4]{0:T(128)} %param.40) | copy-start | bytes 52
  6.5 45.5 %copy-start.9 = (bf16[256,128]{1,0:T(8,128)(2,1)S(1)}, bf16[256,128]{1,0:T(8,128)(2,1)}, u32[]{:S(2)}) copy-start(bf16[256,128]{1,0:T(8,128)(2,1)} %param.33) | copy-start | bytes 196612
  6.6 81.3 %all-gather.26.cloned.1.call-start = ((), (), s32[]{:S(2)}) async-start(), calls=%async_computation.9 | async-start | bytes 1179648 | tf_op jit(solution)/shard_map/all_gather | solution.py:205
  7.3 78.2 %copy-start.15 = (bf16[4,128]{1,0:T(4,128)(2,1)S(1)}, bf16[4,128]{1,0:T(4,128)(2,1)}, u32[]{:S(2)}) copy-start(bf16[4,128]{1,0:T(4,128)(2,1)} %param.38) | copy-start | bytes 3076
  7.3 78.7 %copy-start.12 = (bf16[3,256]{1,0:T(4,128)(2,1)S(1)}, bf16[3,256]{1,0:T(4,128)(2,1)}, u32[]{:S(2)}) copy-start(bf16[3,256]{1,0:T(4,128)(2,1)} %param.35) | copy-start | bytes 4612
  7.3 78.7 %copy-start.20 = (bf16[256]{0:T(256)(128)(2,1)S(1)}, bf16[256]{0:T(256)(128)(2,1)}, u32[]{:S(2)}) copy-start(bf16[256]{0:T(256)(128)(2,1)} %param.43) | copy-start | bytes 1540
  7.3 79.3 %copy-start.21 = (u32[32]{0:T(128)S(1)}, u32[32]{0:T(128)}, u32[]{:S(2)}) copy-start(u32[32]{0:T(128)} %constant.73) | copy-start | bytes 388
  7.3 82.0 %all-gather.12.cloned.1.call-start = ((), (), s32[]{:S(2)}) async-start(), calls=%async_computation.1 | async-start | bytes 2621440 | tf_op jit(solution)/shard_map/all_gather | solution.py:84
  11.4 78.0 %copy-start.10 = (f32[4,512]{1,0:T(4,128)S(1)}, f32[4,512]{1,0:T(4,128)}, u32[]{:S(2)}) copy-start(f32[4,512]{1,0:T(4,128)} %param.41) | copy-start | bytes 24580
  11.4 78.0 %copy-start.17 = (f32[4]{0:T(128)S(1)}, f32[4]{0:T(128)}, u32[]{:S(2)}) copy-start(f32[4]{0:T(128)} %param.39) | copy-start | bytes 52
  11.4 109.0 %all-gather.20.cloned.1.call-start = ((), (), s32[]{:S(2)}) async-start(), calls=%async_computation.5 | async-start | bytes 1179648 | tf_op jit(solution)/shard_map/all_gather | solution.py:91
  12.1 149.3 %all-gather.16.cloned.1.call-start = ((), (), s32[]{:S(2)}) async-start(), calls=%async_computation.3 | async-start | bytes 1179648 | tf_op jit(solution)/shard_map/all_gather | solution.py:88
  12.7 189.7 %all-gather.18.cloned.1.call-start = ((), (), s32[]{:S(2)}) async-start(), calls=%async_computation.4 | async-start | bytes 1179648 | tf_op jit(solution)/shard_map/all_gather | solution.py:89
  13.3 231.1 %all-gather.14.cloned.1.call-start = ((), (), s32[]{:S(2)}) async-start(), calls=%async_computation.2 | async-start | bytes 1179648 | tf_op jit(solution)/shard_map/all_gather | solution.py:87
  13.9 308.4 %all-gather.22.cloned.1.call-start = ((), (), s32[]{:S(2)}) async-start(), calls=%async_computation.6 | async-start | bytes 1179648 | tf_op jit(solution)/shard_map/all_gather | solution.py:90
  14.6 312.8 %all-gather.24.cloned.1.call-start = ((), (), s32[]{:S(2)}) async-start(), calls=%async_computation.7 | async-start | bytes 1179648 | tf_op jit(solution)/shard_map/all_gather | solution.py:206
  15.4 347.0 %reduce-scatter.2.cloned.1.call-start = ((), (), s32[]{:S(2)}) async-start(), calls=%async_computation.8 | async-start | bytes 2621440 | tf_op jit(solution)/shard_map/reduce_scatter | solution.py:208
  89.4 31.0 %copy-start.1 = (bf16[512,2048]{1,0:T(8,128)(2,1)S(1)}, bf16[512,2048]{1,0:T(8,128)(2,1)}, u32[]{:S(2)}) copy-start(bf16[512,2048]{1,0:T(8,128)(2,1)} %all-gather.12.cloned.1.call-done) | copy-start | bytes 6291460
  93.8 0.7 copy-start.2
  120.4 5.3 %copy-start.3 = (bf16[2048,128]{1,0:T(8,128)(2,1)S(1)}, bf16[2048,128]{1,0:T(8,128)(2,1)}, u32[]{:S(2)}) copy-start(bf16[2048,128]{1,0:T(8,128)(2,1)} %all_gather.50) | copy-start | bytes 1572868
  123.2 127.2 %collective-permute-start.2 = (bf16[3,256]{1,0:T(4,128)(2,1)S(1)}, bf16[3,256]{1,0:T(4,128)(2,1)S(1)}, u32[]{:S(2)}, u32[]{:S(2)}) collective-permute-start(bf16[3,256]{1,0:T(4,128)(2,1)S(1)} %slice.137), channel_id=1, source_target_pairs={{0,4},{4,8},{8,12},{12,16},{16,20},{20,24},{24,28},{1,5},{5,9},{9,... | collective-permute-start | bytes 4616 | tf_op jit(solution)/shard_map/ppermute | solution.py:16
  127.7 108.5 %collective-permute-start.3 = (bf16[3,128]{1,0:T(4,128)(2,1)}, bf16[3,128]{1,0:T(4,128)(2,1)}, u32[]{:S(2)}, u32[]{:S(2)}) collective-permute-start(bf16[3,128]{1,0:T(4,128)(2,1)} %slice.145), channel_id=1, source_target_pairs={{0,4},{4,8},{8,12},{12,16},{16,20},{20,24},{24,28},{1,5},{5,9},{9,... | collective-permute-start | bytes 2312 | tf_op jit(solution)/shard_map/ppermute | solution.py:16
  163.3 0.7 copy-start.18
  228.1 10.4 %collective-permute-start.4 = (bf16[3,128]{1,0:T(4,128)(2,1)}, bf16[3,128]{1,0:T(4,128)(2,1)}, u32[]{:S(2)}, u32[]{:S(2)}) collective-permute-start(bf16[3,128]{1,0:T(4,128)(2,1)} %slice.150), channel_id=1, source_target_pairs={{0,4},{4,8},{8,12},{12,16},{16,20},{20,24},{24,28},{1,5},{5,9},{9,... | collective-permute-start | bytes 2312 | tf_op jit(solution)/shard_map/ppermute | solution.py:16
  232.5 11.8 %collective-permute-start.1 = (bf16[2,256]{1,0:T(2,128)(2,1)S(1)}, bf16[2,256]{1,0:T(2,128)(2,1)S(1)}, u32[]{:S(2)}, u32[]{:S(2)}) collective-permute-start(bf16[2,256]{1,0:T(2,128)(2,1)S(1)} %slice.131), channel_id=1, source_target_pairs={{0,4},{4,8},{8,12},{12,16},{16,20},{20,24},{24,28},{1,5},{5,9},{9,... | collective-permute-start | bytes 3080 | tf_op jit(solution)/shard_map/ppermute | solution.py:16
  234.0 10.3 %collective-permute-start = (bf16[2,256]{1,0:T(2,128)(2,1)}, bf16[2,256]{1,0:T(2,128)(2,1)S(1)}, u32[]{:S(2)}, u32[]{:S(2)}) collective-permute-start(bf16[2,256]{1,0:T(2,128)(2,1)} %slice.130), channel_id=1, source_target_pairs={{0,4},{4,8},{8,12},{12,16},{16,20},{20,24},{24,28},{1,5},{5,9},{9,... | collective-permute-start | bytes 3080 | tf_op jit(solution)/shard_map/ppermute | solution.py:16
  238.5 5.8 %copy-start.6 = (f32[512,128]{1,0:T(8,128)}, f32[512,128]{1,0:T(8,128)S(1)}, u32[]{:S(2)}) copy-start(f32[512,128]{1,0:T(8,128)S(1)} %divide_multiply_fusion.2) | copy-start | bytes 786436
  240.9 0.7 copy-start.4
  306.1 10.3 %copy-start.16 = (f32[4]{0:T(128)S(1)}, f32[4]{0:T(128)}, u32[]{:S(2)}) copy-start(f32[4]{0:T(128)} %param.42) | copy-start | bytes 52
  313.8 2.5 copy-start.5
  313.8 2.5 copy-start.7
  324.4 3.0 copy-start.13
Sparse Core Ops, SparseCore 0:
  9.5 44.5 all-gather.25
  55.7 22.2 all-gather.11
  80.1 40.2 all-gather.19
  122.4 38.9 all-gather.15
  163.4 38.9 all-gather.17
  204.4 39.0 all-gather.13
  245.6 41.4 all-gather.21
  289.1 38.2 all-gather.23
  332.2 30.1 reduce-scatter.1
